TPU v7x, 512 devices: a whole 4x4x16 slice. The times are simulated.
512 devices in a mesh: sp: 16 (over z), fs: 4 (over y), tp: 8 (over x, core).
Axes of the slice: x: 4, y: 4, z: 16, core: 2. Of those that a mesh axis runs over, the one named last changes fastest.
Arguments:
- tokens: bfloat16 [4, 4096, 2048], P('fs', 'sp'), may hold values from -6 to 6
- mix_gain: float32 [2048], replicated, may hold values from 0.1 to 1.9
- query_down: bfloat16 [2048, 768], P('fs', 'tp'), may hold values from -0.125 to 0.125
- memory_down: bfloat16 [2048, 512], P('fs', 'tp'), may hold values from -0.125 to 0.125
- rope_weight: bfloat16 [2048, 32], replicated, may hold values from -0.125 to 0.125
- query_up: bfloat16 [768, 1536], P('fs', 'tp'), may hold values from -0.21875 to 0.21875
- key_up: bfloat16 [512, 1024], P('fs', 'tp'), may hold values from -0.25 to 0.25
- value_up: bfloat16 [512, 1024], P('fs', 'tp'), may hold values from -0.25 to 0.25
- latent_gain: float32 [768], replicated, may hold values from 0.1 to 1.9
- memory_gain: float32 [512], replicated, may hold values from 0.1 to 1.9
- query_gain: float32 [96], replicated, may hold values from 1 to 16
- key_gain: float32 [96], replicated, may hold values from 0.1 to 1.9
- conv_value: bfloat16 [2048, 1024], P('fs', 'tp'), may hold values from -1 to 1
- conv_gate: bfloat16 [2048, 1024], P('fs', 'tp'), may hold values from -0.125 to 0.125
- conv_kernel: bfloat16 [31, 1024], P(None, 'tp'), may hold values from -50 to 50
- channel_gain: float32 [1024], P('tp'), may hold values from 0.1 to 1.9
- channel_shift: float32 [1024], P('tp'), may hold values from -3 to 3
- heads_out: bfloat16 [1024, 2048], P('tp', 'fs'), may hold values from -0.75 to 0.75
- conv_out: bfloat16 [1024, 2048], P('tp', 'fs'), may hold values from -0.1875 to 0.1875
Outputs:
- mixed: bfloat16 [4, 4096, 2048], P('fs', 'sp')
All inputs are finite; a program needn't handle non-finite values.
Results may differ from a plain program's by a relative error of at most 0.015.
The roundings to bfloat16 on the way count: a program that leaves them out, or rounds other values in their place, can miss the bound.
Values may be sent and summed in bfloat16 or wider, within the bound.
No kernel may reach another device: no remote copies, remote signals or barrier semaphores. Data moves between devices by JAX's collectives and lax.ppermute only.
A program may use at most 64 MiB of HBM per device.

v0:
```python
import jax
import jax.numpy as jnp
from jax import lax
from jax.experimental import pallas as pl
from jax.experimental.pallas import tpu as pltpu
from jax.sharding import PartitionSpec as P

QK_NOPE = 64
QK_ROPE = 32
V_DIM = 64
CONV_W = 1024
SEG = 64
QK_DIM = 96
Q_LAT = 768
KV_LAT = 512
ROWS = 256
TAPS = 31
HALO = 32
LANES = 128
N_FS = 4
N_TP = 8
N_SP = 16
BUNDLE = 2

epsilon = 1e-06
rope_base = 10000.0
masked_score = -1e30
log2_e = 1.4426950408889634
bf16 = jnp.bfloat16
f32 = jnp.float32

SAME_CORE = [[0, 2, 4, 6], [1, 3, 5, 7]]
CORE_PAIRS = [(i, i ^ 1) for i in range(N_TP)]


def call(kernel, out_shape, scratch=(), scalars=0, arrays=0, specs=None):
    extra = {}
    if scalars:
        smem = pl.BlockSpec(memory_space=pltpu.SMEM)
        specs = [smem] * scalars + [pl.BlockSpec(memory_space=pltpu.VMEM)] * arrays
    if specs:
        extra["in_specs"] = specs
    return pl.pallas_call(
        kernel,
        out_shape=out_shape,
        scratch_shapes=list(scratch),
        compiler_params=pltpu.CompilerParams(vmem_limit_bytes=16 * 1024 * 1024),
        **extra,
    )


def head_tile(tile, gain, cosine, sine_up, sine_down):
    scale = lax.rsqrt(jnp.sum(tile * tile, axis=-1, keepdims=True) * (1.0 / QK_DIM) + epsilon)
    tile = tile * scale * gain
    half = QK_ROPE // 2
    return (
        tile * cosine
        + pltpu.roll(tile, LANES - half, 1) * sine_up
        + pltpu.roll(tile, half, 1) * sine_down
    )


def pack_kernel(qd_ref, md_ref, qu_ref, ku_ref, vu_ref, cv_ref, cg_ref, narrow_ref, wide_ref, qu_scr, sems):
    pairs = [
        (qd_ref, narrow_ref.at[:96, :]),
        (md_ref, narrow_ref.at[96:160, :]),
        (qu_ref, qu_scr),
        (cv_ref, wide_ref.at[:512, :LANES]),
        (cg_ref, wide_ref.at[:512, LANES:]),
    ]
    for n, ref in enumerate((ku_ref, vu_ref)):
        for b in range(2):
            at = (2 * n + b) * LANES
            pairs.append((ref.at[b * 64 : (b + 1) * 64, :], narrow_ref.at[160:, at : at + LANES]))
    copies = [
        pltpu.make_async_copy(source, target, sems.at[n]) for n, (source, target) in enumerate(pairs)
    ]
    for copy in copies:
        copy.start()
    for copy in copies:
        copy.wait()
    wide_ref[512:, :] = jnp.zeros((192, 256), bf16)
    wide_ref[512:, :QK_DIM] = qu_scr[:, :QK_DIM]
    wide_ref[512:, LANES : LANES + QK_DIM] = qu_scr[:, QK_DIM:]


def project_kernel(tok_ref, gain_ref, rope_w_ref, cos_ref, sin_ref, w_ref, lat_ref, rope_ref, normed_ref, cosine_ref, up_ref, down_ref):
    block = 64
    turned = (((1,), (1,)), ((), ()))
    for r in range(0, ROWS, block):
        rows = tok_ref[r : r + block, :].astype(f32)
        scale = lax.rsqrt(jnp.mean(rows * rows, axis=-1, keepdims=True) + epsilon)
        normed_ref[r : r + block, :] = (rows * scale * gain_ref[...]).astype(bf16)
    both = jnp.zeros((ROWS, 160), f32)
    for f in range(N_FS):
        both = both + lax.dot_general(
            normed_ref[:, f * 512 : (f + 1) * 512],
            w_ref[f, :160, :],
            turned,
            preferred_element_type=f32,
        )
    both = both.astype(bf16)
    lat_ref[:ROWS, :] = both[:, :LANES]
    for r in range(4):
        lat_ref[ROWS:, r * 32 : (r + 1) * 32] = both[r * 64 : (r + 1) * 64, LANES:]
    rope = lax.dot_general(normed_ref[...], rope_w_ref[...], turned, preferred_element_type=f32)
    rope_ref[...] = jnp.zeros((ROWS, LANES), bf16)
    rope_ref[:, QK_NOPE:QK_DIM] = rope.astype(bf16)
    half = QK_ROPE // 2
    empty = jnp.zeros((ROWS, LANES - half), f32)
    cosine = jnp.concatenate([cos_ref[...].T, empty], axis=1)
    sine = jnp.concatenate([sin_ref[...].T, empty], axis=1)
    lane = lax.broadcasted_iota(jnp.int32, (ROWS, LANES), 1)
    cosine = pltpu.roll(cosine, QK_NOPE, 1) + pltpu.roll(cosine, QK_NOPE + half, 1)
    cosine_ref[...] = jnp.where(lane < QK_NOPE, 1.0, cosine)
    up_ref[...] = -pltpu.roll(sine, QK_NOPE, 1)
    down_ref[...] = pltpu.roll(sine, QK_NOPE + half, 1)


def keys_values_kernel(lat_ref, rope_ref, w_ref, mgain_ref, kgain_ref, cos_ref, up_ref, down_ref, out_ref, m_scr, w_scr):
    for g in range(N_TP):
        at = g * 64
        m_scr[:, at : at + 32] = lat_ref[g, :ROWS, 96:]
        for r in range(4):
            m_scr[r * 64 : (r + 1) * 64, at + 32 : at + 64] = lat_ref[
                g, ROWS:, r * 32 : (r + 1) * 32
            ]
    raw = m_scr[...].astype(f32)
    scale = lax.rsqrt(jnp.mean(raw * raw, axis=-1, keepdims=True) + epsilon)
    m_scr[...] = (raw * scale * mgain_ref[...]).astype(bf16)
    for f in range(N_FS):
        for n in range(2):
            for b in range(2):
                lanes = (2 * n + b) * LANES
                row = f * 128 + b * 64
                w_scr[row : row + 64, n * LANES : (n + 1) * LANES] = w_ref[
                    f, 160:, lanes : lanes + LANES
                ]
    both = jnp.dot(m_scr[...], w_scr[...], preferred_element_type=f32)
    nope = both[:, :LANES]
    lane = lax.broadcasted_iota(jnp.int32, (ROWS, LANES), 1)
    rope = rope_ref[...].astype(f32)
    tiles = []
    for h in range(2):
        part = nope if h == 0 else pltpu.roll(nope, 64, 1)
        tile = jnp.where(lane < QK_NOPE, part, rope)
        tiles.append(head_tile(tile, kgain_ref[...], cos_ref[...], up_ref[...], down_ref[...]))
    moved = pltpu.roll(tiles[1], QK_DIM, 1)
    values = both[:, LANES:]
    swapped = pltpu.roll(values, V_DIM, 1)
    half = ROWS // 2
    out_ref[:ROWS, :] = jnp.where(lane < QK_DIM, tiles[0], moved).astype(bf16)
    out_ref[ROWS : 2 * ROWS, :] = jnp.where(lane < V_DIM, moved, swapped).astype(bf16)
    out_ref[2 * ROWS :, :] = jnp.where(lane[:half] < V_DIM, swapped[:half], values[half:]).astype(
        bf16
    )


def queries_kernel(lat_ref, w_ref, lgain_ref, qgain_ref, cos_ref, up_ref, down_ref, out_ref, q_scr):
    for g in range(N_TP):
        q_scr[:, g * 96 : (g + 1) * 96] = lat_ref[g, :ROWS, :96]
    raw = q_scr[...].astype(f32)
    scale = lax.rsqrt(jnp.mean(raw * raw, axis=-1, keepdims=True) + epsilon)
    q_scr[...] = (raw * scale * lgain_ref[...]).astype(bf16)
    both = jnp.zeros((ROWS, 2 * LANES), f32)
    for f in range(N_FS):
        both = both + jnp.dot(
            q_scr[:, f * 192 : (f + 1) * 192], w_ref[f, 512:704, :], preferred_element_type=f32
        )
    lane = lax.broadcasted_iota(jnp.int32, (ROWS, LANES), 1)
    tiles = [
        head_tile(
            both[:, h * LANES : (h + 1) * LANES],
            qgain_ref[...],
            cos_ref[...],
            up_ref[...],
            down_ref[...],
        )
        for h in range(2)
    ]
    moved = pltpu.roll(tiles[1], QK_DIM, 1)
    out_ref[:, :LANES] = tiles[0].astype(bf16)
    out_ref[:, LANES : 2 * LANES] = jnp.where(lane < QK_DIM, 0.0, moved).astype(bf16)
    out_ref[:, 2 * LANES :] = jnp.where(lane < V_DIM, moved, 0.0).astype(bf16)


def gated_kernel(normed_ref, w_ref, out_ref):
    both = jnp.zeros((ROWS, 2 * LANES), f32)
    for f in range(N_FS):
        both = both + jnp.dot(
            normed_ref[:, f * 512 : (f + 1) * 512], w_ref[f, :512, :], preferred_element_type=f32
        )
    out_ref[...] = (both[:, :LANES] * jax.nn.sigmoid(both[:, LANES:])).astype(bf16)


def conv_kernel_body(halo_ref, gated_ref, taps_ref, sum_ref, stat_ref, ext_scr):
    ext_scr[:HALO, :] = halo_ref[...].astype(f32)
    ext_scr[HALO:, :] = gated_ref[...].astype(f32)
    start = HALO - (TAPS - 1)
    block = LANES
    stat_ref[4:, :] = jnp.zeros((4, LANES), f32)
    for n in range(ROWS // block):
        r = n * block
        running = jnp.zeros((block, LANES), f32)
        for j in range(TAPS):
            running = running + ext_scr[pl.ds(r + start + j, block), :] * taps_ref[j : j + 1, :]
        sum_ref[r : r + block, :] = running
        flat = running.T
        total = jnp.sum(flat, axis=0, keepdims=True)
        off = flat - total * (1.0 / LANES)
        stat_ref[n : n + 1, :] = total
        stat_ref[2 + n : 3 + n, :] = jnp.sum(off * off, axis=0, keepdims=True)


def channel_kernel(sum_ref, stat_ref, gain_ref, shift_ref, out_ref):
    for n in range(ROWS // LANES):
        total = stat_ref[0, n : n + 1, :]
        for g in range(1, N_TP):
            total = total + stat_ref[g, n : n + 1, :]
        mean = total * (1.0 / CONV_W)
        spread = jnp.zeros((1, LANES), f32)
        for g in range(N_TP):
            apart = stat_ref[g, n : n + 1, :] * (1.0 / LANES) - mean
            spread = spread + stat_ref[g, 2 + n : 3 + n, :] + LANES * apart * apart
        scale = lax.rsqrt(spread * (1.0 / CONV_W) + epsilon)
        mean = jnp.broadcast_to(mean, (LANES, LANES)).T
        scale = jnp.broadcast_to(scale, (LANES, LANES)).T
        rows = slice(n * LANES, (n + 1) * LANES)
        value = (sum_ref[rows, :] - mean) * scale * gain_ref[...] + shift_ref[...]
        out_ref[rows, :] = (value / (1.0 + jnp.exp(-value))).astype(bf16)


def attend(q_ref, blocks, stat, acc, mask=None):
    rate = QK_DIM ** (-0.5) * log2_e
    firsts = [b[:ROWS, :] for b in blocks]
    seconds = [b[ROWS : 2 * ROWS, :] for b in blocks]
    thirds = [b[2 * ROWS :, :] for b in blocks]
    turned = (((1,), (1,)), ((), ()))
    keys_a = jnp.concatenate(firsts, axis=0)
    keys_b = jnp.concatenate(seconds, axis=0)
    score_a = lax.dot_general(q_ref[:, :LANES], keys_a, turned, preferred_element_type=f32)
    score_b = lax.dot_general(
        q_ref[:, LANES:],
        jnp.concatenate([keys_a, keys_b], axis=1),
        turned,
        preferred_element_type=f32,
    )
    for h, scores in enumerate((score_a, score_b)):
        scores = scores * rate
        if mask is not None:
            scores = jnp.where(mask, scores, masked_score)
        top = stat[2 * h]
        new_top = jnp.maximum(top, jnp.max(scores, axis=-1, keepdims=True))
        weights = jnp.exp2(scores - new_top)
        factor = jnp.exp2(top - new_top)
        stat[2 * h] = new_top
        stat[2 * h + 1] = stat[2 * h + 1] * factor + jnp.sum(weights, axis=-1, keepdims=True)
        weights = weights.astype(bf16)
        if h == 0:
            acc[0] = acc[0] * factor + jnp.dot(weights, keys_b, preferred_element_type=f32)
        else:
            left = acc[1] * factor
            right = acc[2] * factor
            for n, third in enumerate(thirds):
                at = n * ROWS
                half = ROWS // 2
                left = left + jnp.dot(
                    weights[:, at : at + half], third, preferred_element_type=f32
                )
                right = right + jnp.dot(
                    weights[:, at + half : at + ROWS], third, preferred_element_type=f32
                )
            acc[1] = left
            acc[2] = right


def attention_kernel(at_ref, q_ref, kv_ref, conv_ref, heads_ref, conv_w_ref, out_ref, kv, stat, acc, sems):
    at = at_ref[0]
    copies = [
        pltpu.make_async_copy(kv_ref.at[n], kv.at[n], sems.at[n]) for n in range(N_SP // BUNDLE)
    ]
    for copy in copies:
        copy.start()
    for h in range(2):
        stat[2 * h] = jnp.full((ROWS, 1), masked_score, f32)
        stat[2 * h + 1] = jnp.zeros((ROWS, 1), f32)
    acc[...] = jnp.zeros(acc.shape, f32)
    wide = BUNDLE * ROWS
    for n, copy in enumerate(copies):
        copy.wait()
        blocks = [kv.at[n, i] for i in range(BUNDLE)]

        def whole(blocks=blocks):
            attend(q_ref, blocks, stat, acc)

        def cut(blocks=blocks, n=n):
            row = lax.broadcasted_iota(jnp.int32, (ROWS, wide), 0) + at * ROWS
            col = lax.broadcasted_iota(jnp.int32, (ROWS, wide), 1) + n * wide
            mask = jnp.right_shift(col, 6) <= jnp.right_shift(row, 6)
            attend(q_ref, blocks, stat, acc, mask)

        pl.when(at >= (n + 1) * BUNDLE)(whole)
        pl.when(jnp.logical_and(at >= n * BUNDLE, at < (n + 1) * BUNDLE))(cut)
    lane = lax.broadcasted_iota(jnp.int32, (ROWS, LANES), 1)
    result = jnp.where(
        lane < V_DIM,
        pltpu.roll(acc[0], V_DIM, 1) / stat[1],
        (pltpu.roll(acc[1], V_DIM, 1) + acc[2]) / stat[3],
    ).astype(bf16)
    conv = conv_ref[...]
    share = ROWS // N_TP
    for f in range(N_FS):
        part = (
            jnp.dot(result, heads_ref[f], preferred_element_type=f32)
            + jnp.dot(conv, conv_w_ref[f], preferred_element_type=f32)
        ).astype(bf16)
        for r in range(N_TP):
            out_ref[r, :, f * 512 : (f + 1) * 512] = part[r * share : (r + 1) * share]


def total_kernel(in_ref, out_ref):
    total = in_ref[0].astype(f32)
    for g in range(1, N_TP):
        total = total + in_ref[g].astype(f32)
    out_ref[...] = total.astype(bf16)


def assemble_kernel(core_ref, mine_ref, other_ref, out_ref):
    share = ROWS // N_TP

    def place(first, second):
        for x in range(N_TP // 2):
            out_ref[2 * x * share : (2 * x + 1) * share, :] = first[x]
            out_ref[(2 * x + 1) * share : (2 * x + 2) * share, :] = second[x]

    pl.when(core_ref[0] == 0)(lambda: place(mine_ref, other_ref))
    pl.when(core_ref[0] == 1)(lambda: place(other_ref, mine_ref))


def rotation_tables(positions):
    inverse_freq = 1.0 / rope_base ** (jnp.arange(0, QK_ROPE, 2, dtype=f32) / QK_ROPE)
    angles = positions.astype(f32)[None, :] * inverse_freq[:, None]
    return jnp.cos(angles), jnp.sin(angles)


def local(
    tokens,
    mix_gain,
    query_down,
    memory_down,
    rope_weight,
    query_up,
    key_up,
    value_up,
    latent_gain,
    memory_gain,
    query_gain,
    key_gain,
    conv_value,
    conv_gate,
    conv_kernel,
    channel_gain,
    channel_shift,
    heads_out,
    conv_out,
):
    at = lax.axis_index("sp")
    hbm = pl.BlockSpec(memory_space=pltpu.HBM)
    vmem = pl.BlockSpec(memory_space=pltpu.VMEM)
    narrow, wide = call(
        pack_kernel,
        (jax.ShapeDtypeStruct((224, 512), bf16), jax.ShapeDtypeStruct((704, 256), bf16)),
        [pltpu.VMEM((192, 192), bf16), pltpu.SemaphoreType.DMA((9,))],
        specs=[hbm] * 7,
    )(
        *(
            pltpu.with_memory_space_constraint(a, pltpu.HBM)
            for a in (
                query_down.T, memory_down.T, query_up, key_up, value_up, conv_value, conv_gate
            )
        )
    )
    wide_all = lax.all_gather(wide, "fs")
    narrow_all = lax.all_gather(narrow, "fs")
    positions = at * ROWS + jnp.arange(ROWS, dtype=jnp.int32)
    cosine, sine = rotation_tables(positions)
    table = jax.ShapeDtypeStruct((ROWS, LANES), f32)
    latents, rope_rows, normed, cosine, sine_up, sine_down = call(
        project_kernel,
        (
            jax.ShapeDtypeStruct((320, LANES), bf16),
            jax.ShapeDtypeStruct((ROWS, LANES), bf16),
            jax.ShapeDtypeStruct((ROWS, 2048), bf16),
            table,
            table,
            table,
        ),
    )(tokens[0], mix_gain[None, :], rope_weight.T, cosine, sine, narrow_all)
    latents = lax.all_gather(latents, "tp")

    def row(vector, width):
        return jnp.pad(vector, (0, width - vector.shape[0]))[None, :]

    own = call(
        keys_values_kernel,
        jax.ShapeDtypeStruct((5 * LANES, LANES), bf16),
        [pltpu.VMEM((ROWS, KV_LAT), bf16), pltpu.VMEM((KV_LAT, 256), bf16)],
    )(
        latents, rope_rows, narrow_all, memory_gain[None, :], row(key_gain, LANES),
        cosine, sine_up, sine_down,
    )
    pieces = lax.all_gather(own, "sp")
    queries = call(
        queries_kernel,
        jax.ShapeDtypeStruct((ROWS, 3 * LANES), bf16),
        [pltpu.VMEM((ROWS, Q_LAT), bf16)],
    )(
        latents, wide_all, latent_gain[None, :], row(query_gain, LANES),
        cosine, sine_up, sine_down,
    )
    gated = call(gated_kernel, jax.ShapeDtypeStruct((ROWS, LANES), bf16))(normed, wide_all)
    halo = lax.ppermute(gated[ROWS - HALO :], "sp", [(i, i + 1) for i in range(N_SP - 1)])
    taps = jnp.pad(conv_kernel.astype(f32), ((0, 1), (0, 0)))
    conv_sum, stats = call(
        conv_kernel_body,
        (jax.ShapeDtypeStruct((ROWS, LANES), f32), jax.ShapeDtypeStruct((8, LANES), f32)),
        [pltpu.VMEM((ROWS + HALO, LANES), f32)],
    )(halo, gated, taps)
    stats = lax.all_gather(stats, "tp")
    conv_result = call(channel_kernel, jax.ShapeDtypeStruct((ROWS, LANES), bf16))(
        conv_sum, stats, channel_gain[None, :], channel_shift[None, :]
    )
    heads_all = lax.all_gather(heads_out, "fs")
    conv_all = lax.all_gather(conv_out, "fs")
    core = jnp.bitwise_and(lax.axis_index("tp"), 1)[None]
    pieces = pltpu.with_memory_space_constraint(
        pieces.reshape(N_SP // BUNDLE, BUNDLE, 5 * LANES, LANES), pltpu.HBM
    )
    partial = call(
        attention_kernel,
        jax.ShapeDtypeStruct((N_TP, ROWS // N_TP, 2048), bf16),
        [
            pltpu.VMEM((N_SP // BUNDLE, BUNDLE, 5 * LANES, LANES), bf16),
            pltpu.VMEM((4, ROWS, 1), f32),
            pltpu.VMEM((3, ROWS, LANES), f32),
            pltpu.SemaphoreType.DMA((N_SP // BUNDLE,)),
        ],
        specs=[
            pl.BlockSpec(memory_space=pltpu.SMEM), vmem, hbm, vmem, vmem, vmem,
        ],
    )(at[None], queries, pieces, conv_result, heads_all, conv_all)
    share = lax.all_to_all(partial, "tp", split_axis=0, concat_axis=0, tiled=True)
    share = call(total_kernel, jax.ShapeDtypeStruct((ROWS // N_TP, 2048), bf16))(share)
    mine = lax.all_gather(share, "tp", axis_index_groups=SAME_CORE)
    other = lax.ppermute(mine, "tp", CORE_PAIRS)
    mixed = call(
        assemble_kernel, jax.ShapeDtypeStruct((ROWS, 2048), bf16), scalars=1, arrays=2
    )(core, mine, other)
    return mixed[None]


def solution(mesh):
    in_specs = (
        P("fs", "sp", None),
        P(),
        P("fs", "tp"),
        P("fs", "tp"),
        P(),
        P("fs", "tp"),
        P("fs", "tp"),
        P("fs", "tp"),
        P(),
        P(),
        P(),
        P(),
        P("fs", "tp"),
        P("fs", "tp"),
        P(None, "tp"),
        P("tp"),
        P("tp"),
        P("tp", "fs"),
        P("tp", "fs"),
    )
    out_specs = P("fs", "sp", None)
    return jax.shard_map(local, mesh=mesh, in_specs=in_specs, out_specs=out_specs, check_vma=False)
```

profile of v0, /device:TPU:1, one launch (start us, length us, event | category | flops | bytes accessed | tf_op | source)
XLA Modules:
  0.0 173.4 jit_solution(1453103270041065138)
XLA Ops:
  6.5 0.0 copy-start.1
  6.5 0.0 copy-start.11
  6.5 0.0 copy-start.4
  6.5 0.0 all-gather.11.cloned.1.call-start
  6.5 2.1 %shard_map.181 = (bf16[224,512]{1,0:T(8,128)(2,1)S(1)}, bf16[704,256]{1,0:T(8,128)(2,1)}) custom-call(bf16[96,512]{1,0:T(8,128)(2,1)} %bitcast.41, bf16[64,512]{1,0:T(8,128)(2,1)} %bitcast.42, bf16[192,192]{1,0:T(8,128)(2,1)} %qu_ref.1, bf16[128,128]{1,0:T(8,128)(2,1)} %ku_ref.1, bf16[128,128]{1,0:T(8,128)(2,1)} %vu_ref.1, bf16[512,128]{1,0:T(8,128)(2,1)} %cv_ref.1, ...), custom_call_target="tpu_custom_call" | custom-call | tf_op jit(solution)/shard_map/pallas_call | solution.py:370
  8.6 0.0 all-gather.11.cloned.1.call-update
  8.7 0.0 all-gather.13.cloned.1.call-start
  8.8 0.1 multiply_sine_fusion
  8.9 12.8 %all-gather = bf16[896,512]{1,0:T(8,128)(2,1)S(1)} all-gather(bf16[224,512]{1,0:T(8,128)(2,1)S(1)} %get-tuple-element.15), channel_id=2, replica_groups=mesh['sp'=16,'fs'=4,'tp'=8] {'fs'}, dimensions={0}, use_global_device_ids=true | all-gather | bytes 1146880 | tf_op jit(solution)/shard_map/all_gather | solution.py:384
  21.7 0.0 copy-done.1
  21.7 0.0 copy-start.2
  21.7 0.9 copy-done.2
  22.6 0.0 copy-start.3
  22.6 0.7 copy-done.3
  23.3 0.0 copy-start.9
  23.3 0.0 copy-start.7
  23.3 0.0 copy-start.8
  23.3 1.0 shard_map.182
  24.3 0.0 copy-done.11
  24.4 21.2 %all-gather.1 = bf16[2560,128]{1,0:T(8,128)(2,1)S(1)} all-gather(bf16[320,128]{1,0:T(8,128)(2,1)S(1)} %get-tuple-element.16), channel_id=3, replica_groups=mesh['sp'=16,'fs'=4,'tp'=8] {'tp'}, dimensions={0}, use_global_device_ids=true | all-gather | bytes 737280 | tf_op jit(solution)/shard_map/all_gather | solution.py:399
  45.5 0.0 copy-done.4
  45.5 0.0 copy-start.12
  45.5 0.0 copy-start.10
  45.5 2.1 %shard_map.184 = bf16[640,128]{1,0:T(8,128)(2,1)} custom-call(bf16[8,320,128]{2,1,0:T(8,128)(2,1)S(1)} %bitcast.25, bf16[256,128]{1,0:T(8,128)(2,1)S(1)} %get-tuple-element.21.rope_ref, bf16[4,224,512]{2,1,0:T(8,128)(2,1)S(1)} %bitcast.24, f32[1,512]{1,0:T(1,128)S(1)} %bitcast.37, f32[1,128]{1,0:T(1,128)S(1)} %pad_bitcast_fusion.kgain_ref, ...), custom_call_target="tpu_custom_call" | custom-call | tf_op jit(solution)/shard_map/pallas_call | solution.py:404
  47.6 0.0 all-gather.13.cloned.1.call-update
  47.7 0.0 copy-done.9
  47.7 0.0 copy-done.7
  47.7 10.3 %all-gather.5 = bf16[512,512]{1,0:T(8,128)(2,1)S(1)} all-gather(bf16[128,512]{1,0:T(8,128)(2,1)S(1)} %copy-done.7), channel_id=7, replica_groups=mesh['sp'=16,'fs'=4,'tp'=8] {'fs'}, dimensions={0}, use_global_device_ids=true | all-gather | bytes 655360 | tf_op jit(solution)/shard_map/all_gather | solution.py:433
  58.0 0.0 copy-done.8
  58.0 11.2 %all-gather.6 = bf16[512,512]{1,0:T(8,128)(2,1)S(1)} all-gather(bf16[128,512]{1,0:T(8,128)(2,1)S(1)} %copy-done.8), channel_id=8, replica_groups=mesh['sp'=16,'fs'=4,'tp'=8] {'fs'}, dimensions={0}, use_global_device_ids=true | all-gather | bytes 655360 | tf_op jit(solution)/shard_map/all_gather | solution.py:434
  69.2 0.0 all-gather.11.cloned.1.call-done
  69.2 0.0 copy-start
  69.2 1.4 copy-done
  70.6 0.0 copy-start.5
  70.6 0.0 copy-start.6
  70.6 0.4 shard_map.185.gated_ref
  71.0 1.3 collective-permute-start
  72.3 0.0 copy-done.12
  72.3 0.0 copy-done.10
  72.4 1.2 shard_map.183.q_ref
  73.6 0.0 collective-permute-done.halo_ref
  73.6 0.4 shard_map.186
  74.0 17.8 %all-gather.4 = f32[64,128]{1,0:T(8,128)S(1)} all-gather(f32[8,128]{1,0:T(8,128)S(1)} %get-tuple-element.24), channel_id=6, replica_groups=mesh['sp'=16,'fs'=4,'tp'=8] {'tp'}, dimensions={0}, use_global_device_ids=true | all-gather | bytes 36864 | tf_op jit(solution)/shard_map/all_gather | solution.py:429
  91.8 0.0 copy-done.5
  91.8 0.0 copy-done.6
  91.8 0.2 shard_map.187.conv_ref
  92.0 23.2 %all-gather.13.cloned.1.call-done = bf16[10240,128]{1,0:T(8,128)(2,1)} async-done(((bf16[640,128]{1,0:T(8,128)(2,1)}), bf16[10240,128]{1,0:T(8,128)(2,1)}) %all-gather.13.cloned.1.call-update) | async-done | bytes 2621456 | tf_op jit(solution)/shard_map/all_gather | solution.py:412
  115.2 3.4 %shard_map.188 = bf16[8,32,2048]{2,1,0:T(8,128)(2,1)S(1)} custom-call(s32[1]{0:T(128)} %bitcast.1.at_ref, bf16[256,384]{1,0:T(8,128)(2,1)S(1)} %shard_map.183.q_ref, bf16[8,2,640,128]{3,2,1,0:T(8,128)(2,1)} %bitcast.40, bf16[256,128]{1,0:T(8,128)(2,1)S(1)} %shard_map.187.conv_ref, bf16[4,128,512]{2,1,0:T(8,128)(2,1)S(1)} %bitcast.29, ...), custom_call_target="tpu_custom_call" | custom-call | tf_op jit(solution)/shard_map/pallas_call | solution.py:439
  118.6 29.0 %all_to_all.5.in_ref = bf16[8,32,2048]{2,1,0:T(8,128)(2,1)S(1)} all-to-all(bf16[8,32,2048]{2,1,0:T(8,128)(2,1)S(1)} %shard_map.188), channel_id=1, replica_groups=mesh['sp'=16,'fs'=4,'tp'=8] {'tp'}, dimensions={0} | all-to-all | bytes 2097152 | tf_op jit(solution)/shard_map/all_to_all | solution.py:452
  147.6 0.1 shard_map.189
  147.7 10.1 %all-gather.7 = bf16[128,2048]{1,0:T(8,128)(2,1)S(1)} all-gather(bf16[32,2048]{1,0:T(8,128)(2,1)S(1)} %shard_map.189), channel_id=9, replica_groups={{0,2,4,6},{1,3,5,7},{8,10,12,14},{9,11,13,15},{16,18,20,22},{17,19,21,2..., dimensions={0}, use_global_device_ids=true | all-gather | bytes 655360 | tf_op jit(solution)/shard_map/all_gather | solution.py:454
  157.7 6.3 %collective-permute-start.1 = (bf16[4,32,2048]{2,1,0:T(8,128)(2,1)S(1)}, bf16[4,32,2048]{2,1,0:T(8,128)(2,1)S(1)}, u32[]{:S(2)}, u32[]{:S(2)}) collective-permute-start(bf16[4,32,2048]{2,1,0:T(8,128)(2,1)S(1)} %bitcast.31), channel_id=1, source_target_pairs={{0,1},{1,0},{2,3},{3,2},{4,5},{5,4},{6,7},{7,6},{8,9},{9,8},{10,11... | collective-permute-start | bytes 1572872 | tf_op jit(solution)/shard_map/ppermute | solution.py:455
  164.0 1.5 collective-permute-done.1.other_ref
  165.5 1.0 shard_map.190
  (7 shorter events, 0.0 us)
Async XLA Ops:
  6.5 15.1 %copy-start.1 = (bf16[1,256,2048]{2,1,0:T(8,128)(2,1)S(1)}, bf16[1,256,2048]{2,1,0:T(8,128)(2,1)}, u32[]{:S(2)}) copy-start(bf16[1,256,2048]{2,1,0:T(8,128)(2,1)} %param.19) | copy-start | bytes 3145732
  6.5 17.8 %copy-start.11 = (f32[96]{0:T(128)S(1)}, f32[96]{0:T(128)}, u32[]{:S(2)}) copy-start(f32[96]{0:T(128)} %param.30) | copy-start | bytes 1156
  6.5 39.0 %copy-start.4 = (f32[512]{0:T(512)S(1)}, f32[512]{0:T(512)}, u32[]{:S(2)}) copy-start(f32[512]{0:T(512)} %param.28) | copy-start | bytes 6148
  6.5 62.7 %all-gather.11.cloned.1.call-start = ((), (), s32[]{:S(2)}) async-start(), calls=%async_computation.1 | async-start | bytes 1802240 | tf_op jit(solution)/shard_map/all_gather | solution.py:383
  8.7 106.5 %all-gather.13.cloned.1.call-start = ((), (), s32[]{:S(2)}) async-start(), calls=%async_computation.2 | async-start | bytes 2785280 | tf_op jit(solution)/shard_map/all_gather | solution.py:412
  21.7 0.9 copy-start.2
  22.6 0.7 copy-start.3
  23.3 24.4 %copy-start.9 = (bf16[31,128]{1,0:T(8,128)(2,1)S(1)}, bf16[31,128]{1,0:T(8,128)(2,1)}, u32[]{:S(2)}) copy-start(bf16[31,128]{1,0:T(8,128)(2,1)} %param.33) | copy-start | bytes 23812
  23.3 24.4 %copy-start.7 = (bf16[128,512]{1,0:T(8,128)(2,1)S(1)}, bf16[128,512]{1,0:T(8,128)(2,1)}, u32[]{:S(2)}) copy-start(bf16[128,512]{1,0:T(8,128)(2,1)} %param.36) | copy-start | bytes 393220
  23.3 34.7 %copy-start.8 = (bf16[128,512]{1,0:T(8,128)(2,1)S(1)}, bf16[128,512]{1,0:T(8,128)(2,1)}, u32[]{:S(2)}) copy-start(bf16[128,512]{1,0:T(8,128)(2,1)} %param.37) | copy-start | bytes 393220
  45.5 26.8 %copy-start.12 = (f32[96]{0:T(128)S(1)}, f32[96]{0:T(128)}, u32[]{:S(2)}) copy-start(f32[96]{0:T(128)} %param.29) | copy-start | bytes 1156
  45.5 26.8 %copy-start.10 = (f32[768]{0:T(1024)S(1)}, f32[768]{0:T(1024)}, u32[]{:S(2)}) copy-start(f32[768]{0:T(1024)} %param.27) | copy-start | bytes 9220
  69.2 1.4 copy-start
  70.6 21.2 %copy-start.5 = (f32[128]{0:T(128)S(1)}, f32[128]{0:T(128)}, u32[]{:S(2)}) copy-start(f32[128]{0:T(128)} %param.34) | copy-start | bytes 1540
  70.6 21.2 %copy-start.6 = (f32[128]{0:T(128)S(1)}, f32[128]{0:T(128)}, u32[]{:S(2)}) copy-start(f32[128]{0:T(128)} %param.35) | copy-start | bytes 1540
  71.0 2.5 %collective-permute-start = (bf16[32,128]{1,0:T(8,128)(2,1)S(1)}, bf16[32,128]{1,0:T(8,128)(2,1)S(1)}, u32[]{:S(2)}, u32[]{:S(2)}) collective-permute-start(bf16[32,128]{1,0:T(8,128)(2,1)S(1)} %slice.4), channel_id=1, source_target_pairs={{0,32},{32,64},{64,96},{96,128},{128,160},{160,192},{192,224},{224... | collective-permute-start | bytes 24584 | tf_op jit(solution)/shard_map/ppermute | solution.py:422
  157.7 7.8 %collective-permute-start.1 = (bf16[4,32,2048]{2,1,0:T(8,128)(2,1)S(1)}, bf16[4,32,2048]{2,1,0:T(8,128)(2,1)S(1)}, u32[]{:S(2)}, u32[]{:S(2)}) collective-permute-start(bf16[4,32,2048]{2,1,0:T(8,128)(2,1)S(1)} %bitcast.31), channel_id=1, source_target_pairs={{0,1},{1,0},{2,3},{3,2},{4,5},{5,4},{6,7},{7,6},{8,9},{9,8},{10,11... | collective-permute-start | bytes 1572872 | tf_op jit(solution)/shard_map/ppermute | solution.py:455
Sparse Core Ops, SparseCore 0:
  9.4 38.1 all-gather.10
  49.8 65.4 all-gather.12
where the time goes:
time: 176 us; the launch traced here: 173 us
  blocking collectives  112 us (64%)
  waiting for transfers between devices  24.8 us (14%)
  between operations  13.6 us (8%)
  Pallas kernels  12 us (7%)
  starting transfers between devices  7.6 us (4%)
  local copies, waits for them, and re-layouts  3.02 us (2%)
    all_to_all x1, blocking collectives, local(): lax.all_to_all(partial, 'tp', split_axis=0, concat_axis=0, tiled=True)  29 us
    all_gather x1, waiting for transfers between devices, local(): pieces = lax.all_gather(own, 'sp')  23.2 us
    all_gather x1, blocking collectives, local(): latents = lax.all_gather(latents, 'tp')  21.2 us
    all_gather x1, blocking collectives, local(): stats = lax.all_gather(stats, 'tp')  17.8 us
    all_gather x1, blocking collectives, local(): narrow_all = lax.all_gather(narrow, 'fs')  12.8 us
    all_gather x1, blocking collectives, local(): conv_all = lax.all_gather(conv_out, 'fs')  11.2 us
    all_gather x1, blocking collectives, local(): heads_all = lax.all_gather(heads_out, 'fs')  10.3 us
    all_gather x1, blocking collectives, local(): mine = lax.all_gather(share, 'tp', axis_index_groups=SAME_CORE)  10.1 us
  transfers between devices with their start and end apart: 4, of which 2 were waited for; matrix products, arithmetic and copies ran while one was open for 0% of the time, Pallas kernels for 3%

commit v1 on v0

--- a/solution.py
+++ b/solution.py
@@ -20,7 +20,7 @@
 N_FS = 4
 N_TP = 8
 N_SP = 16
-BUNDLE = 2
+BUNDLE = 4
 
 epsilon = 1e-06
 rope_base = 10000.0
@@ -60,13 +60,15 @@
     )
 
 
-def pack_kernel(qd_ref, md_ref, qu_ref, ku_ref, vu_ref, cv_ref, cg_ref, narrow_ref, wide_ref, qu_scr, sems):
+def pack_kernel(qd_ref, md_ref, qu_ref, ku_ref, vu_ref, cv_ref, cg_ref, rope_ref, gain_ref, narrow_ref, wide_ref, rope_out, gain_out, qu_scr, sems):
     pairs = [
         (qd_ref, narrow_ref.at[:96, :]),
         (md_ref, narrow_ref.at[96:160, :]),
         (qu_ref, qu_scr),
         (cv_ref, wide_ref.at[:512, :LANES]),
         (cg_ref, wide_ref.at[:512, LANES:]),
+        (rope_ref, rope_out),
+        (gain_ref, gain_out),
     ]
     for n, ref in enumerate((ku_ref, vu_ref)):
         for b in range(2):
@@ -84,11 +86,19 @@
     wide_ref[512:, LANES : LANES + QK_DIM] = qu_scr[:, QK_DIM:]
 
 
-def project_kernel(tok_ref, gain_ref, rope_w_ref, cos_ref, sin_ref, w_ref, lat_ref, rope_ref, normed_ref, cosine_ref, up_ref, down_ref):
+def project_kernel(tok_ref, gain_ref, rope_w_ref, cos_ref, sin_ref, w_ref, lat_ref, rope_ref, normed_ref, cosine_ref, up_ref, down_ref, tok_scr, sems):
     block = 64
+    copies = []
+    for n in range(ROWS // block):
+        rows = slice(n * block, (n + 1) * block)
+        copies.append(
+            pltpu.make_async_copy(tok_ref.at[rows, :], tok_scr.at[rows, :], sems.at[n])
+        )
+        copies[-1].start()
     turned = (((1,), (1,)), ((), ()))
     for r in range(0, ROWS, block):
-        rows = tok_ref[r : r + block, :].astype(f32)
+        copies[r // block].wait()
+        rows = tok_scr[r : r + block, :].astype(f32)
         scale = lax.rsqrt(jnp.mean(rows * rows, axis=-1, keepdims=True) + epsilon)
         normed_ref[r : r + block, :] = (rows * scale * gain_ref[...]).astype(bf16)
     both = jnp.zeros((ROWS, 160), f32)
@@ -145,15 +155,12 @@
         part = nope if h == 0 else pltpu.roll(nope, 64, 1)
         tile = jnp.where(lane < QK_NOPE, part, rope)
         tiles.append(head_tile(tile, kgain_ref[...], cos_ref[...], up_ref[...], down_ref[...]))
-    moved = pltpu.roll(tiles[1], QK_DIM, 1)
-    values = both[:, LANES:]
-    swapped = pltpu.roll(values, V_DIM, 1)
-    half = ROWS // 2
-    out_ref[:ROWS, :] = jnp.where(lane < QK_DIM, tiles[0], moved).astype(bf16)
-    out_ref[ROWS : 2 * ROWS, :] = jnp.where(lane < V_DIM, moved, swapped).astype(bf16)
-    out_ref[2 * ROWS :, :] = jnp.where(lane[:half] < V_DIM, swapped[:half], values[half:]).astype(
-        bf16
-    )
+    for h in range(2):
+        out_ref[h * ROWS : (h + 1) * ROWS, :] = tiles[h].astype(bf16)
+    values = both[:, LANES:].T.astype(bf16)
+    for half in range(2):
+        at = 2 * ROWS + half * LANES
+        out_ref[at : at + LANES, :] = values[:, half * LANES : (half + 1) * LANES]
 
 
 def queries_kernel(lat_ref, w_ref, lgain_ref, qgain_ref, cos_ref, up_ref, down_ref, out_ref, q_scr):
@@ -178,10 +185,8 @@
         )
         for h in range(2)
     ]
-    moved = pltpu.roll(tiles[1], QK_DIM, 1)
-    out_ref[:, :LANES] = tiles[0].astype(bf16)
-    out_ref[:, LANES : 2 * LANES] = jnp.where(lane < QK_DIM, 0.0, moved).astype(bf16)
-    out_ref[:, 2 * LANES :] = jnp.where(lane < V_DIM, moved, 0.0).astype(bf16)
+    for h in range(2):
+        out_ref[:, h * LANES : (h + 1) * LANES] = tiles[h].astype(bf16)
 
 
 def gated_kernel(normed_ref, w_ref, out_ref):
@@ -230,83 +235,82 @@
         out_ref[rows, :] = (value / (1.0 + jnp.exp(-value))).astype(bf16)
 
 
-def attend(q_ref, blocks, stat, acc, mask=None):
+def attend(q_ref, blocks, state, hidden, mask=None):
     rate = QK_DIM ** (-0.5) * log2_e
-    firsts = [b[:ROWS, :] for b in blocks]
-    seconds = [b[ROWS : 2 * ROWS, :] for b in blocks]
-    thirds = [b[2 * ROWS :, :] for b in blocks]
-    turned = (((1,), (1,)), ((), ()))
-    keys_a = jnp.concatenate(firsts, axis=0)
-    keys_b = jnp.concatenate(seconds, axis=0)
-    score_a = lax.dot_general(q_ref[:, :LANES], keys_a, turned, preferred_element_type=f32)
-    score_b = lax.dot_general(
-        q_ref[:, LANES:],
-        jnp.concatenate([keys_a, keys_b], axis=1),
-        turned,
-        preferred_element_type=f32,
-    )
-    for h, scores in enumerate((score_a, score_b)):
-        scores = scores * rate
+    fresh = []
+    for h in range(2):
+        top, total, weighted = state[h]
+        keys = jnp.concatenate([b[h * ROWS : (h + 1) * ROWS, :] for b in blocks], axis=0)
+        scores = lax.dot_general(
+            keys,
+            q_ref[:, h * LANES : (h + 1) * LANES],
+            (((1,), (1,)), ((), ())),
+            preferred_element_type=f32,
+        )
         if mask is not None:
             scores = jnp.where(mask, scores, masked_score)
-        top = stat[2 * h]
-        new_top = jnp.maximum(top, jnp.max(scores, axis=-1, keepdims=True))
-        weights = jnp.exp2(scores - new_top)
-        factor = jnp.exp2(top - new_top)
-        stat[2 * h] = new_top
-        stat[2 * h + 1] = stat[2 * h + 1] * factor + jnp.sum(weights, axis=-1, keepdims=True)
-        weights = weights.astype(bf16)
-        if h == 0:
-            acc[0] = acc[0] * factor + jnp.dot(weights, keys_b, preferred_element_type=f32)
-        else:
-            left = acc[1] * factor
-            right = acc[2] * factor
-            for n, third in enumerate(thirds):
-                at = n * ROWS
-                half = ROWS // 2
-                left = left + jnp.dot(
-                    weights[:, at : at + half], third, preferred_element_type=f32
-                )
-                right = right + jnp.dot(
-                    weights[:, at + half : at + ROWS], third, preferred_element_type=f32
-                )
-            acc[1] = left
-            acc[2] = right
-
-
-def attention_kernel(at_ref, q_ref, kv_ref, conv_ref, heads_ref, conv_w_ref, out_ref, kv, stat, acc, sems):
+        new_top = top
+        for n, off in enumerate(hidden):
+            part = jnp.max(scores[n * ROWS : (n + 1) * ROWS], axis=0, keepdims=True)
+            new_top = jnp.maximum(new_top, part - off)
+        weights = jnp.concatenate(
+            [
+                jnp.exp2(scores[n * ROWS : (n + 1) * ROWS] * rate - (new_top * rate + off))
+                for n, off in enumerate(hidden)
+            ],
+            axis=0,
+        )
+        factor = jnp.exp2((top - new_top) * rate)
+        total = total * factor + jnp.sum(weights, axis=0, keepdims=True)
+        at = 2 * ROWS + h * V_DIM
+        values = jnp.concatenate(
+            [b[at + i * LANES : at + i * LANES + V_DIM, :] for b in blocks for i in range(2)],
+            axis=1,
+        )
+        weighted = weighted * factor + jnp.dot(
+            values, weights.astype(bf16), preferred_element_type=f32
+        )
+        fresh.append((new_top, total, weighted))
+    return fresh
+
+
+def own_kernel(q_ref, own_ref, stat_ref, acc_ref):
+    key = lax.broadcasted_iota(jnp.int32, (ROWS, ROWS), 0)
+    query = lax.broadcasted_iota(jnp.int32, (ROWS, ROWS), 1)
+    mask = jnp.right_shift(key, 6) <= jnp.right_shift(query, 6)
+    empty = (
+        jnp.full((1, ROWS), masked_score, f32),
+        jnp.zeros((1, ROWS), f32),
+        jnp.zeros((V_DIM, ROWS), f32),
+    )
+    state = attend(q_ref, [own_ref], [empty, empty], [0.0], mask)
+    stat_ref[4:, :] = jnp.zeros((4, ROWS), f32)
+    for h in range(2):
+        stat_ref[2 * h : 2 * h + 1, :] = state[h][0]
+        stat_ref[2 * h + 1 : 2 * h + 2, :] = state[h][1]
+        acc_ref[h * V_DIM : (h + 1) * V_DIM, :] = state[h][2]
+
+
+def attention_kernel(at_ref, q_ref, kv_ref, stat_ref, acc_ref, conv_ref, heads_ref, conv_w_ref, out_ref, kv, sems):
     at = at_ref[0]
     copies = [
         pltpu.make_async_copy(kv_ref.at[n], kv.at[n], sems.at[n]) for n in range(N_SP // BUNDLE)
     ]
     for copy in copies:
         copy.start()
-    for h in range(2):
-        stat[2 * h] = jnp.full((ROWS, 1), masked_score, f32)
-        stat[2 * h + 1] = jnp.zeros((ROWS, 1), f32)
-    acc[...] = jnp.zeros(acc.shape, f32)
-    wide = BUNDLE * ROWS
+    state = [
+        (
+            stat_ref[2 * h : 2 * h + 1, :],
+            stat_ref[2 * h + 1 : 2 * h + 2, :],
+            acc_ref[h * V_DIM : (h + 1) * V_DIM, :],
+        )
+        for h in range(2)
+    ]
     for n, copy in enumerate(copies):
         copy.wait()
-        blocks = [kv.at[n, i] for i in range(BUNDLE)]
-
-        def whole(blocks=blocks):
-            attend(q_ref, blocks, stat, acc)
-
-        def cut(blocks=blocks, n=n):
-            row = lax.broadcasted_iota(jnp.int32, (ROWS, wide), 0) + at * ROWS
-            col = lax.broadcasted_iota(jnp.int32, (ROWS, wide), 1) + n * wide
-            mask = jnp.right_shift(col, 6) <= jnp.right_shift(row, 6)
-            attend(q_ref, blocks, stat, acc, mask)
-
-        pl.when(at >= (n + 1) * BUNDLE)(whole)
-        pl.when(jnp.logical_and(at >= n * BUNDLE, at < (n + 1) * BUNDLE))(cut)
-    lane = lax.broadcasted_iota(jnp.int32, (ROWS, LANES), 1)
-    result = jnp.where(
-        lane < V_DIM,
-        pltpu.roll(acc[0], V_DIM, 1) / stat[1],
-        (pltpu.roll(acc[1], V_DIM, 1) + acc[2]) / stat[3],
-    ).astype(bf16)
+        hidden = [jnp.where(n * BUNDLE + i < at, 0.0, -masked_score) for i in range(BUNDLE)]
+        state = attend(q_ref, [kv.at[n, i] for i in range(BUNDLE)], state, hidden)
+    result = jnp.concatenate([state[h][2] / state[h][1] for h in range(2)], axis=0).T.astype(bf16)
     conv = conv_ref[...]
     share = ROWS // N_TP
     for f in range(N_FS):
@@ -367,16 +371,22 @@
     at = lax.axis_index("sp")
     hbm = pl.BlockSpec(memory_space=pltpu.HBM)
     vmem = pl.BlockSpec(memory_space=pltpu.VMEM)
-    narrow, wide = call(
+    narrow, wide, rope_w, gain = call(
         pack_kernel,
-        (jax.ShapeDtypeStruct((224, 512), bf16), jax.ShapeDtypeStruct((704, 256), bf16)),
-        [pltpu.VMEM((192, 192), bf16), pltpu.SemaphoreType.DMA((9,))],
-        specs=[hbm] * 7,
+        (
+            jax.ShapeDtypeStruct((224, 512), bf16),
+            jax.ShapeDtypeStruct((704, 256), bf16),
+            jax.ShapeDtypeStruct((QK_ROPE, 2048), bf16),
+            jax.ShapeDtypeStruct((1, 2048), f32),
+        ),
+        [pltpu.VMEM((192, 192), bf16), pltpu.SemaphoreType.DMA((11,))],
+        specs=[hbm] * 9,
     )(
         *(
             pltpu.with_memory_space_constraint(a, pltpu.HBM)
             for a in (
-                query_down.T, memory_down.T, query_up, key_up, value_up, conv_value, conv_gate
+                query_down.T, memory_down.T, query_up, key_up, value_up, conv_value, conv_gate,
+                rope_weight.T, mix_gain[None, :],
             )
         )
     )
@@ -395,7 +405,9 @@
             table,
             table,
         ),
-    )(tokens[0], mix_gain[None, :], rope_weight.T, cosine, sine, narrow_all)
+        [pltpu.VMEM((ROWS, 2048), bf16), pltpu.SemaphoreType.DMA((4,))],
+        specs=[hbm] + [vmem] * 5,
+    )(pltpu.with_memory_space_constraint(tokens[0], pltpu.HBM), gain, rope_w, cosine, sine, narrow_all)
     latents = lax.all_gather(latents, "tp")
 
     def row(vector, width):
@@ -403,7 +415,7 @@
 
     own = call(
         keys_values_kernel,
-        jax.ShapeDtypeStruct((5 * LANES, LANES), bf16),
+        jax.ShapeDtypeStruct((6 * LANES, LANES), bf16),
         [pltpu.VMEM((ROWS, KV_LAT), bf16), pltpu.VMEM((KV_LAT, 256), bf16)],
     )(
         latents, rope_rows, narrow_all, memory_gain[None, :], row(key_gain, LANES),
@@ -412,7 +424,7 @@
     pieces = lax.all_gather(own, "sp")
     queries = call(
         queries_kernel,
-        jax.ShapeDtypeStruct((ROWS, 3 * LANES), bf16),
+        jax.ShapeDtypeStruct((ROWS, 2 * LANES), bf16),
         [pltpu.VMEM((ROWS, Q_LAT), bf16)],
     )(
         latents, wide_all, latent_gain[None, :], row(query_gain, LANES),
@@ -430,25 +442,27 @@
     conv_result = call(channel_kernel, jax.ShapeDtypeStruct((ROWS, LANES), bf16))(
         conv_sum, stats, channel_gain[None, :], channel_shift[None, :]
     )
+    stat, acc = call(
+        own_kernel,
+        (jax.ShapeDtypeStruct((8, ROWS), f32), jax.ShapeDtypeStruct((2 * V_DIM, ROWS), f32)),
+    )(queries, own)
     heads_all = lax.all_gather(heads_out, "fs")
     conv_all = lax.all_gather(conv_out, "fs")
     core = jnp.bitwise_and(lax.axis_index("tp"), 1)[None]
     pieces = pltpu.with_memory_space_constraint(
-        pieces.reshape(N_SP // BUNDLE, BUNDLE, 5 * LANES, LANES), pltpu.HBM
+        pieces.reshape(N_SP // BUNDLE, BUNDLE, 6 * LANES, LANES), pltpu.HBM
     )
     partial = call(
         attention_kernel,
         jax.ShapeDtypeStruct((N_TP, ROWS // N_TP, 2048), bf16),
         [
-            pltpu.VMEM((N_SP // BUNDLE, BUNDLE, 5 * LANES, LANES), bf16),
-            pltpu.VMEM((4, ROWS, 1), f32),
-            pltpu.VMEM((3, ROWS, LANES), f32),
+            pltpu.VMEM((N_SP // BUNDLE, BUNDLE, 6 * LANES, LANES), bf16),
             pltpu.SemaphoreType.DMA((N_SP // BUNDLE,)),
         ],
         specs=[
-            pl.BlockSpec(memory_space=pltpu.SMEM), vmem, hbm, vmem, vmem, vmem,
+            pl.BlockSpec(memory_space=pltpu.SMEM), vmem, hbm, vmem, vmem, vmem, vmem, vmem,
         ],
-    )(at[None], queries, pieces, conv_result, heads_all, conv_all)
+    )(at[None], queries, pieces, stat, acc, conv_result, heads_all, conv_all)
     share = lax.all_to_all(partial, "tp", split_axis=0, concat_axis=0, tiled=True)
     share = call(total_kernel, jax.ShapeDtypeStruct((ROWS // N_TP, 2048), bf16))(share)
     mine = lax.all_gather(share, "tp", axis_index_groups=SAME_CORE)

time: 176 us -> 179 us (1.017); the launches traced: 173 us -> 179 us
  Pallas kernels: 12 us -> 19.2 us
    pallas_call x1, Pallas kernels: 3.38 us -> 7.7 us  [local(): call(attention_kernel, jax.ShapeDtypeStruct((N_TP, ROWS // N_TP, 2048), b...]
    pallas_call x2 -> x3, Pallas kernels: 3.28 us -> 4.87 us  [the longest x1 2.08 us: local(): call(keys_values_kernel, jax.ShapeDtypeStruct((6 * LANES, LANES), bf16),...]
  transfers between devices with their start and end apart: 4 -> 4, of which waited for: 2 -> 2; matrix products, arithmetic and copies ran while one was open for 0% -> 0% of each run, Pallas kernels for 3% -> 5%
where the time goes in v1:
time: 179 us
  blocking collectives  112 us (63%)
  waiting for transfers between devices  25 us (14%)
  Pallas kernels  19.2 us (11%)
  between operations  13.6 us (8%)
  starting transfers between devices  7.6 us (4%)
    all_to_all x1, blocking collectives, local(): lax.all_to_all(partial, 'tp', split_axis=0, concat_axis=0, tiled=True)  28.6 us
    all_gather x1, waiting for transfers between devices, local(): pieces = lax.all_gather(own, 'sp')  23.4 us
    all_gather x1, blocking collectives, local(): latents = lax.all_gather(latents, 'tp')  21.2 us
    all_gather x1, blocking collectives, local(): stats = lax.all_gather(stats, 'tp')  17.7 us
    all_gather x1, blocking collectives, local(): narrow_all = lax.all_gather(narrow, 'fs')  12.9 us
    all_gather x1, blocking collectives, local(): conv_all = lax.all_gather(conv_out, 'fs')  11.4 us
    all_gather x1, blocking collectives, local(): heads_all = lax.all_gather(heads_out, 'fs')  10.3 us
    all_gather x1, blocking collectives, local(): mine = lax.all_gather(share, 'tp', axis_index_groups=SAME_CORE)  10.1 us
  transfers between devices with their start and end apart: 4, of which 2 were waited for; matrix products, arithmetic and copies ran while one was open for 0% of the time, Pallas kernels for 5%

profile of v1, /device:TPU:1, one launch (start us, length us, event | category | flops | bytes accessed | tf_op | source)
XLA Modules:
  0.0 179.1 jit_solution(10279435753367913960)
XLA Ops:
  6.5 0.0 copy-start.8
  6.5 0.0 copy-start.1
  6.5 0.0 all-gather.11.cloned.1.call-start
  6.5 2.1 %shard_map.181 = (bf16[224,512]{1,0:T(8,128)(2,1)S(1)}, bf16[704,256]{1,0:T(8,128)(2,1)}, bf16[32,2048]{1,0:T(8,128)(2,1)S(1)}, f32[1,2048]{1,0:T(1,128)S(1)}) custom-call(bf16[96,512]{1,0:T(8,128)(2,1)} %bitcast.40, bf16[64,512]{1,0:T(8,128)(2,1)} %bitcast.41, bf16[192,192]{1,0:T(8,128)(2,1)} %qu_ref.1, bf16[128,128]{1,0:T(8,128)(2,1)} %ku_ref.1, ...), custom_call_target="tpu_custom_call" | custom-call | tf_op jit(solution)/shard_map/pallas_call | solution.py:374
  8.7 0.0 all-gather.11.cloned.1.call-update
  8.7 0.0 all-gather.13.cloned.1.call-start
  8.8 0.1 multiply_sine_fusion
  8.9 0.0 copy-start.6
  8.9 0.0 copy-start.4
  8.9 12.9 %all-gather = bf16[896,512]{1,0:T(8,128)(2,1)S(1)} all-gather(bf16[224,512]{1,0:T(8,128)(2,1)S(1)} %get-tuple-element.21), channel_id=2, replica_groups=mesh['sp'=16,'fs'=4,'tp'=8] {'fs'}, dimensions={0}, use_global_device_ids=true | all-gather | bytes 1146880 | tf_op jit(solution)/shard_map/all_gather | solution.py:394
  21.8 0.0 copy-start.5
  21.8 2.3 %shard_map.182 = (bf16[320,128]{1,0:T(8,128)(2,1)S(1)}, bf16[256,128]{1,0:T(8,128)(2,1)S(1)}, bf16[256,2048]{1,0:T(8,128)(2,1)S(1)}, f32[256,128]{1,0:T(8,128)S(...) custom-call(bf16[256,2048]{1,0:T(8,128)(2,1)} %bitcast.38, f32[1,2048]{1,0:T(1,128)S(1)} %get-tuple-element.19.gain_ref, ...), custom_call_target="tpu_custom_call" | custom-call | tf_op jit(solution)/shard_map/pallas_call | solution.py:398
  24.2 0.0 copy-done.8
  24.2 21.2 %all-gather.1 = bf16[2560,128]{1,0:T(8,128)(2,1)S(1)} all-gather(bf16[320,128]{1,0:T(8,128)(2,1)S(1)} %get-tuple-element.22), channel_id=3, replica_groups=mesh['sp'=16,'fs'=4,'tp'=8] {'tp'}, dimensions={0}, use_global_device_ids=true | all-gather | bytes 737280 | tf_op jit(solution)/shard_map/all_gather | solution.py:411
  45.4 0.0 copy-done.1
  45.4 0.0 copy-start.9
  45.4 0.0 copy-start.7
  45.4 2.1 %shard_map.184.own_ref = bf16[768,128]{1,0:T(8,128)(2,1)} custom-call(bf16[8,320,128]{2,1,0:T(8,128)(2,1)S(1)} %bitcast.25, bf16[256,128]{1,0:T(8,128)(2,1)S(1)} %get-tuple-element.27.rope_ref, bf16[4,224,512]{2,1,0:T(8,128)(2,1)S(1)} %bitcast.24, f32[1,512]{1,0:T(1,128)S(1)} %bitcast.34, f32[1,128]{1,0:T(1,128)S(1)} %pad_bitcast_fusion.kgain_ref, ...), custom_call_target="tpu_custom_call" | custom-call | tf_op jit(solution)/shard_map/pallas_call | solution.py:416
  47.5 0.0 all-gather.13.cloned.1.call-update
  47.5 0.0 copy-done.6
  47.5 0.0 copy-done.4
  47.6 10.3 %all-gather.5 = bf16[512,512]{1,0:T(8,128)(2,1)S(1)} all-gather(bf16[128,512]{1,0:T(8,128)(2,1)S(1)} %copy-done.4), channel_id=7, replica_groups=mesh['sp'=16,'fs'=4,'tp'=8] {'fs'}, dimensions={0}, use_global_device_ids=true | all-gather | bytes 655360 | tf_op jit(solution)/shard_map/all_gather | solution.py:449
  57.8 0.0 copy-done.5
  57.8 0.0 copy-start.2
  57.8 0.0 copy-start.3
  57.8 11.4 %all-gather.6 = bf16[512,512]{1,0:T(8,128)(2,1)S(1)} all-gather(bf16[128,512]{1,0:T(8,128)(2,1)S(1)} %copy-done.5), channel_id=8, replica_groups=mesh['sp'=16,'fs'=4,'tp'=8] {'fs'}, dimensions={0}, use_global_device_ids=true | all-gather | bytes 655360 | tf_op jit(solution)/shard_map/all_gather | solution.py:450
  69.2 0.0 all-gather.11.cloned.1.call-done
  69.2 0.0 copy-start
  69.2 1.4 copy-done
  70.6 0.4 shard_map.186.gated_ref
  71.0 1.3 collective-permute-start
  72.3 0.0 copy-done.9
  72.3 0.0 copy-done.7
  72.4 1.1 shard_map.183.q_ref
  73.5 1.7 shard_map.185
  75.2 0.0 collective-permute-done.halo_ref
  75.2 0.4 shard_map.187
  75.6 17.7 %all-gather.4 = f32[64,128]{1,0:T(8,128)S(1)} all-gather(f32[8,128]{1,0:T(8,128)S(1)} %get-tuple-element.32), channel_id=6, replica_groups=mesh['sp'=16,'fs'=4,'tp'=8] {'tp'}, dimensions={0}, use_global_device_ids=true | all-gather | bytes 36864 | tf_op jit(solution)/shard_map/all_gather | solution.py:441
  93.3 0.0 copy-done.2
  93.3 0.0 copy-done.3
  93.3 0.2 shard_map.188.conv_ref
  93.5 23.4 %all-gather.13.cloned.1.call-done = bf16[12288,128]{1,0:T(8,128)(2,1)} async-done(((bf16[768,128]{1,0:T(8,128)(2,1)}), bf16[12288,128]{1,0:T(8,128)(2,1)}) %all-gather.13.cloned.1.call-update) | async-done | bytes 3145744 | tf_op jit(solution)/shard_map/all_gather | solution.py:424
  117.0 7.7 %shard_map.189 = bf16[8,32,2048]{2,1,0:T(8,128)(2,1)S(1)} custom-call(s32[1]{0:T(128)} %bitcast.1.at_ref, bf16[256,256]{1,0:T(8,128)(2,1)S(1)} %shard_map.183.q_ref, bf16[4,4,768,128]{3,2,1,0:T(8,128)(2,1)} %bitcast.37, f32[8,256]{1,0:T(8,128)S(1)} %get-tuple-element.28.stat_ref, f32[128,256]{1,0:T(8,128)S(1)} %get-tuple-element.29.acc_ref, ...), custom_call_target="tpu_custom_call" | custom-call | tf_op jit(solution)/shard_map/pallas_call | solution.py:455
  124.7 28.6 %all_to_all.5.in_ref = bf16[8,32,2048]{2,1,0:T(8,128)(2,1)S(1)} all-to-all(bf16[8,32,2048]{2,1,0:T(8,128)(2,1)S(1)} %shard_map.189), channel_id=1, replica_groups=mesh['sp'=16,'fs'=4,'tp'=8] {'tp'}, dimensions={0} | all-to-all | bytes 2097152 | tf_op jit(solution)/shard_map/all_to_all | solution.py:466
  153.3 0.1 shard_map.190
  153.4 10.1 %all-gather.7 = bf16[128,2048]{1,0:T(8,128)(2,1)S(1)} all-gather(bf16[32,2048]{1,0:T(8,128)(2,1)S(1)} %shard_map.190), channel_id=9, replica_groups={{0,2,4,6},{1,3,5,7},{8,10,12,14},{9,11,13,15},{16,18,20,22},{17,19,21,2..., dimensions={0}, use_global_device_ids=true | all-gather | bytes 655360 | tf_op jit(solution)/shard_map/all_gather | solution.py:468
  163.4 6.3 %collective-permute-start.1 = (bf16[4,32,2048]{2,1,0:T(8,128)(2,1)S(1)}, bf16[4,32,2048]{2,1,0:T(8,128)(2,1)S(1)}, u32[]{:S(2)}, u32[]{:S(2)}) collective-permute-start(bf16[4,32,2048]{2,1,0:T(8,128)(2,1)S(1)} %bitcast.31), channel_id=1, source_target_pairs={{0,1},{1,0},{2,3},{3,2},{4,5},{5,4},{6,7},{7,6},{8,9},{9,8},{10,11... | collective-permute-start | bytes 1572872 | tf_op jit(solution)/shard_map/ppermute | solution.py:469
  169.7 1.5 collective-permute-done.1.other_ref
  171.2 1.0 shard_map.191
  (7 shorter events, 0.0 us)
Async XLA Ops:
  6.5 17.7 %copy-start.8 = (f32[96]{0:T(128)S(1)}, f32[96]{0:T(128)}, u32[]{:S(2)}) copy-start(f32[96]{0:T(128)} %param.30) | copy-start | bytes 1156
  6.5 38.9 %copy-start.1 = (f32[512]{0:T(512)S(1)}, f32[512]{0:T(512)}, u32[]{:S(2)}) copy-start(f32[512]{0:T(512)} %param.28) | copy-start | bytes 6148
  6.5 62.7 %all-gather.11.cloned.1.call-start = ((), (), s32[]{:S(2)}) async-start(), calls=%async_computation.1 | async-start | bytes 1802240 | tf_op jit(solution)/shard_map/all_gather | solution.py:393
  8.7 108.3 %all-gather.13.cloned.1.call-start = ((), (), s32[]{:S(2)}) async-start(), calls=%async_computation.2 | async-start | bytes 3342336 | tf_op jit(solution)/shard_map/all_gather | solution.py:424
  8.9 38.6 %copy-start.6 = (bf16[31,128]{1,0:T(8,128)(2,1)S(1)}, bf16[31,128]{1,0:T(8,128)(2,1)}, u32[]{:S(2)}) copy-start(bf16[31,128]{1,0:T(8,128)(2,1)} %param.33) | copy-start | bytes 23812
  8.9 38.6 %copy-start.4 = (bf16[128,512]{1,0:T(8,128)(2,1)S(1)}, bf16[128,512]{1,0:T(8,128)(2,1)}, u32[]{:S(2)}) copy-start(bf16[128,512]{1,0:T(8,128)(2,1)} %param.36) | copy-start | bytes 393220
  21.8 36.0 %copy-start.5 = (bf16[128,512]{1,0:T(8,128)(2,1)S(1)}, bf16[128,512]{1,0:T(8,128)(2,1)}, u32[]{:S(2)}) copy-start(bf16[128,512]{1,0:T(8,128)(2,1)} %param.37) | copy-start | bytes 393220
  45.4 26.9 %copy-start.9 = (f32[96]{0:T(128)S(1)}, f32[96]{0:T(128)}, u32[]{:S(2)}) copy-start(f32[96]{0:T(128)} %param.29) | copy-start | bytes 1156
  45.4 26.9 %copy-start.7 = (f32[768]{0:T(1024)S(1)}, f32[768]{0:T(1024)}, u32[]{:S(2)}) copy-start(f32[768]{0:T(1024)} %param.27) | copy-start | bytes 9220
  57.8 35.5 %copy-start.2 = (f32[128]{0:T(128)S(1)}, f32[128]{0:T(128)}, u32[]{:S(2)}) copy-start(f32[128]{0:T(128)} %param.34) | copy-start | bytes 1540
  57.8 35.5 %copy-start.3 = (f32[128]{0:T(128)S(1)}, f32[128]{0:T(128)}, u32[]{:S(2)}) copy-start(f32[128]{0:T(128)} %param.35) | copy-start | bytes 1540
  69.2 1.4 copy-start
  71.0 4.1 %collective-permute-start = (bf16[32,128]{1,0:T(8,128)(2,1)S(1)}, bf16[32,128]{1,0:T(8,128)(2,1)S(1)}, u32[]{:S(2)}, u32[]{:S(2)}) collective-permute-start(bf16[32,128]{1,0:T(8,128)(2,1)S(1)} %slice.4), channel_id=1, source_target_pairs={{0,32},{32,64},{64,96},{96,128},{128,160},{160,192},{192,224},{224... | collective-permute-start | bytes 24584 | tf_op jit(solution)/shard_map/ppermute | solution.py:434
  163.4 7.8 %collective-permute-start.1 = (bf16[4,32,2048]{2,1,0:T(8,128)(2,1)S(1)}, bf16[4,32,2048]{2,1,0:T(8,128)(2,1)S(1)}, u32[]{:S(2)}, u32[]{:S(2)}) collective-permute-start(bf16[4,32,2048]{2,1,0:T(8,128)(2,1)S(1)} %bitcast.31), channel_id=1, source_target_pairs={{0,1},{1,0},{2,3},{3,2},{4,5},{5,4},{6,7},{7,6},{8,9},{9,8},{10,11... | collective-permute-start | bytes 1572872 | tf_op jit(solution)/shard_map/ppermute | solution.py:469
Sparse Core Ops, SparseCore 0:
  9.4 38.1 all-gather.10
  49.7 67.1 all-gather.12

commit v2 on v1

--- a/solution.py
+++ b/solution.py
@@ -60,13 +60,20 @@
     )
 
 
-def pack_kernel(qd_ref, md_ref, qu_ref, ku_ref, vu_ref, cv_ref, cg_ref, rope_ref, gain_ref, narrow_ref, wide_ref, rope_out, gain_out, qu_scr, sems):
+def copy_all(pairs, sems):
+    copies = [
+        pltpu.make_async_copy(source, target, sems.at[n]) for n, (source, target) in enumerate(pairs)
+    ]
+    for copy in copies:
+        copy.start()
+    for copy in copies:
+        copy.wait()
+
+
+def pack_kernel(qd_ref, md_ref, ku_ref, vu_ref, rope_ref, gain_ref, narrow_ref, rope_out, gain_out, sems):
     pairs = [
         (qd_ref, narrow_ref.at[:96, :]),
         (md_ref, narrow_ref.at[96:160, :]),
-        (qu_ref, qu_scr),
-        (cv_ref, wide_ref.at[:512, :LANES]),
-        (cg_ref, wide_ref.at[:512, LANES:]),
         (rope_ref, rope_out),
         (gain_ref, gain_out),
     ]
@@ -74,16 +81,28 @@
         for b in range(2):
             at = (2 * n + b) * LANES
             pairs.append((ref.at[b * 64 : (b + 1) * 64, :], narrow_ref.at[160:, at : at + LANES]))
-    copies = [
-        pltpu.make_async_copy(source, target, sems.at[n]) for n, (source, target) in enumerate(pairs)
+    copy_all(pairs, sems)
+
+
+def pack_rest_kernel(qu_ref, cv_ref, cg_ref, ho_ref, co_ref, first_ref, second_ref, third_ref, qu_scr, sems):
+    pairs = [
+        (qu_ref, qu_scr),
+        (ho_ref.at[:64, :], second_ref.at[128:, :]),
+        (ho_ref.at[64:, :], third_ref.at[:64, :]),
+        (co_ref, third_ref.at[64:, :]),
     ]
-    for copy in copies:
-        copy.start()
-    for copy in copies:
-        copy.wait()
-    wide_ref[512:, :] = jnp.zeros((192, 256), bf16)
-    wide_ref[512:, :QK_DIM] = qu_scr[:, :QK_DIM]
-    wide_ref[512:, LANES : LANES + QK_DIM] = qu_scr[:, QK_DIM:]
+    for ref, out in ((cv_ref, first_ref), (cg_ref, second_ref)):
+        for b in range(4):
+            rows = slice(b * 128, (b + 1) * 128)
+            pairs.append((ref.at[rows, :], out.at[:128, rows]))
+    copy_all(pairs, sems)
+    first_ref[128:, :] = jnp.zeros((96, 512), bf16)
+    for half in range(2):
+        for h in range(2):
+            at = half * 256 + h * LANES
+            first_ref[128:, at : at + QK_DIM] = qu_scr[
+                half * 96 : (half + 1) * 96, h * QK_DIM : (h + 1) * QK_DIM
+            ]
 
 
 def project_kernel(tok_ref, gain_ref, rope_w_ref, cos_ref, sin_ref, w_ref, lat_ref, rope_ref, normed_ref, cosine_ref, up_ref, down_ref, tok_scr, sems):
@@ -171,9 +190,13 @@
     q_scr[...] = (raw * scale * lgain_ref[...]).astype(bf16)
     both = jnp.zeros((ROWS, 2 * LANES), f32)
     for f in range(N_FS):
-        both = both + jnp.dot(
-            q_scr[:, f * 192 : (f + 1) * 192], w_ref[f, 512:704, :], preferred_element_type=f32
-        )
+        for half in range(2):
+            at = f * 192 + half * 96
+            both = both + jnp.dot(
+                q_scr[:, at : at + 96],
+                w_ref[f, 128:, half * 256 : (half + 1) * 256],
+                preferred_element_type=f32,
+            )
     lane = lax.broadcasted_iota(jnp.int32, (ROWS, LANES), 1)
     tiles = [
         head_tile(
@@ -189,13 +212,16 @@
         out_ref[:, h * LANES : (h + 1) * LANES] = tiles[h].astype(bf16)
 
 
-def gated_kernel(normed_ref, w_ref, out_ref):
-    both = jnp.zeros((ROWS, 2 * LANES), f32)
+def gated_kernel(normed_ref, value_ref, gate_ref, out_ref):
+    value = jnp.zeros((ROWS, LANES), f32)
+    gate = jnp.zeros((ROWS, LANES), f32)
     for f in range(N_FS):
-        both = both + jnp.dot(
-            normed_ref[:, f * 512 : (f + 1) * 512], w_ref[f, :512, :], preferred_element_type=f32
-        )
-    out_ref[...] = (both[:, :LANES] * jax.nn.sigmoid(both[:, LANES:])).astype(bf16)
+        for b in range(4):
+            rows = normed_ref[:, f * 512 + b * LANES : f * 512 + (b + 1) * LANES]
+            cols = slice(b * LANES, (b + 1) * LANES)
+            value = value + jnp.dot(rows, value_ref[f, :128, cols], preferred_element_type=f32)
+            gate = gate + jnp.dot(rows, gate_ref[f, :128, cols], preferred_element_type=f32)
+    out_ref[...] = (value * jax.nn.sigmoid(gate)).astype(bf16)
 
 
 def conv_kernel_body(halo_ref, gated_ref, taps_ref, sum_ref, stat_ref, ext_scr):
@@ -291,7 +317,7 @@
         acc_ref[h * V_DIM : (h + 1) * V_DIM, :] = state[h][2]
 
 
-def attention_kernel(at_ref, q_ref, kv_ref, stat_ref, acc_ref, conv_ref, heads_ref, conv_w_ref, out_ref, kv, sems):
+def attention_kernel(at_ref, q_ref, kv_ref, stat_ref, acc_ref, conv_ref, second_ref, third_ref, out_ref, kv, sems):
     at = at_ref[0]
     copies = [
         pltpu.make_async_copy(kv_ref.at[n], kv.at[n], sems.at[n]) for n in range(N_SP // BUNDLE)
@@ -309,15 +335,19 @@
     for n, copy in enumerate(copies):
         copy.wait()
         hidden = [jnp.where(n * BUNDLE + i < at, 0.0, -masked_score) for i in range(BUNDLE)]
-        state = attend(q_ref, [kv.at[n, i] for i in range(BUNDLE)], state, hidden)
+        blocks = [kv.at[n, i] for i in range(BUNDLE)]
+        state = lax.cond(
+            n * BUNDLE < at,
+            lambda s, blocks=blocks, hidden=hidden: attend(q_ref, blocks, s, hidden),
+            lambda s: s,
+            state,
+        )
     result = jnp.concatenate([state[h][2] / state[h][1] for h in range(2)], axis=0).T.astype(bf16)
-    conv = conv_ref[...]
+    result = jnp.concatenate([result, conv_ref[...]], axis=1)
     share = ROWS // N_TP
     for f in range(N_FS):
-        part = (
-            jnp.dot(result, heads_ref[f], preferred_element_type=f32)
-            + jnp.dot(conv, conv_w_ref[f], preferred_element_type=f32)
-        ).astype(bf16)
+        weight = jnp.concatenate([second_ref[f, 128:, :], third_ref[f]], axis=0)
+        part = jnp.dot(result, weight, preferred_element_type=f32).astype(bf16)
         for r in range(N_TP):
             out_ref[r, :, f * 512 : (f + 1) * 512] = part[r * share : (r + 1) * share]
 
@@ -371,26 +401,23 @@
     at = lax.axis_index("sp")
     hbm = pl.BlockSpec(memory_space=pltpu.HBM)
     vmem = pl.BlockSpec(memory_space=pltpu.VMEM)
-    narrow, wide, rope_w, gain = call(
+    def kept(*arrays):
+        return [pltpu.with_memory_space_constraint(a, pltpu.HBM) for a in arrays]
+
+    narrow, rope_w, gain = call(
         pack_kernel,
         (
             jax.ShapeDtypeStruct((224, 512), bf16),
-            jax.ShapeDtypeStruct((704, 256), bf16),
             jax.ShapeDtypeStruct((QK_ROPE, 2048), bf16),
             jax.ShapeDtypeStruct((1, 2048), f32),
         ),
-        [pltpu.VMEM((192, 192), bf16), pltpu.SemaphoreType.DMA((11,))],
-        specs=[hbm] * 9,
+        [pltpu.SemaphoreType.DMA((8,))],
+        specs=[hbm] * 6,
     )(
-        *(
-            pltpu.with_memory_space_constraint(a, pltpu.HBM)
-            for a in (
-                query_down.T, memory_down.T, query_up, key_up, value_up, conv_value, conv_gate,
-                rope_weight.T, mix_gain[None, :],
-            )
-        )
-    )
-    wide_all = lax.all_gather(wide, "fs")
+        *kept(
+            query_down.T, memory_down.T, key_up, value_up, rope_weight.T, mix_gain[None, :]
+        )
+    )
     narrow_all = lax.all_gather(narrow, "fs")
     positions = at * ROWS + jnp.arange(ROWS, dtype=jnp.int32)
     cosine, sine = rotation_tables(positions)
@@ -421,16 +448,26 @@
         latents, rope_rows, narrow_all, memory_gain[None, :], row(key_gain, LANES),
         cosine, sine_up, sine_down,
     )
+    own, *rest = lax.optimization_barrier(
+        (own, query_up, conv_value, conv_gate, heads_out, conv_out)
+    )
     pieces = lax.all_gather(own, "sp")
+    packed = call(
+        pack_rest_kernel,
+        tuple(jax.ShapeDtypeStruct((rows, 512), bf16) for rows in (224, 192, 192)),
+        [pltpu.VMEM((192, 192), bf16), pltpu.SemaphoreType.DMA((12,))],
+        specs=[hbm] * 5,
+    )(*kept(*rest))
+    first_all, second_all = (lax.all_gather(p, "fs") for p in packed[:2])
     queries = call(
         queries_kernel,
         jax.ShapeDtypeStruct((ROWS, 2 * LANES), bf16),
         [pltpu.VMEM((ROWS, Q_LAT), bf16)],
     )(
-        latents, wide_all, latent_gain[None, :], row(query_gain, LANES),
+        latents, first_all, latent_gain[None, :], row(query_gain, LANES),
         cosine, sine_up, sine_down,
     )
-    gated = call(gated_kernel, jax.ShapeDtypeStruct((ROWS, LANES), bf16))(normed, wide_all)
+    gated = call(gated_kernel, jax.ShapeDtypeStruct((ROWS, LANES), bf16))(normed, first_all, second_all)
     halo = lax.ppermute(gated[ROWS - HALO :], "sp", [(i, i + 1) for i in range(N_SP - 1)])
     taps = jnp.pad(conv_kernel.astype(f32), ((0, 1), (0, 0)))
     conv_sum, stats = call(
@@ -446,8 +483,7 @@
         own_kernel,
         (jax.ShapeDtypeStruct((8, ROWS), f32), jax.ShapeDtypeStruct((2 * V_DIM, ROWS), f32)),
     )(queries, own)
-    heads_all = lax.all_gather(heads_out, "fs")
-    conv_all = lax.all_gather(conv_out, "fs")
+    third_all = lax.all_gather(packed[2], "fs")
     core = jnp.bitwise_and(lax.axis_index("tp"), 1)[None]
     pieces = pltpu.with_memory_space_constraint(
         pieces.reshape(N_SP // BUNDLE, BUNDLE, 6 * LANES, LANES), pltpu.HBM
@@ -462,7 +498,7 @@
         specs=[
             pl.BlockSpec(memory_space=pltpu.SMEM), vmem, hbm, vmem, vmem, vmem, vmem, vmem,
         ],
-    )(at[None], queries, pieces, stat, acc, conv_result, heads_all, conv_all)
+    )(at[None], queries, pieces, stat, acc, conv_result, second_all, third_all)
     share = lax.all_to_all(partial, "tp", split_axis=0, concat_axis=0, tiled=True)
     share = call(total_kernel, jax.ShapeDtypeStruct((ROWS // N_TP, 2048), bf16))(share)
     mine = lax.all_gather(share, "tp", axis_index_groups=SAME_CORE)

time: 179 us -> 169 us (0.944)
  waiting for transfers between devices: 25 us -> 6.03 us
  blocking collectives: 112 us -> 127 us
  Pallas kernels: 19.2 us -> 14.5 us
    all_gather x1, waiting for transfers between devices: 23.4 us -> 4.5 us  [local(): pieces = lax.all_gather(own, 'sp')]
    all_gather x2 -> x3, blocking collectives: 21.6 us -> 35.1 us  [the longest x2 24 us: local(): first_all, second_all = (lax.all_gather(p, 'fs') for p in packed[:2])]
    pallas_call x1, Pallas kernels: 7.7 us -> 2.37 us  [local(): call(attention_kernel, jax.ShapeDtypeStruct((N_TP, ROWS // N_TP, 2048), b...]
  transfers between devices with their start and end apart: 4 -> 3, of which waited for: 2 -> 2; matrix products, arithmetic and copies ran while one was open for 0% -> 0% of each run, Pallas kernels for 5% -> 3%
where the time goes in v2:
time: 169 us
  blocking collectives  127 us (75%)
  Pallas kernels  14.5 us (9%)
  between operations  13.6 us (8%)
  starting transfers between devices  7.56 us (4%)
  waiting for transfers between devices  6.03 us (4%)
    all_to_all x1, blocking collectives, local(): lax.all_to_all(partial, 'tp', split_axis=0, concat_axis=0, tiled=True)  28.4 us
    all_gather x2, blocking collectives, local(): first_all, second_all = (lax.all_gather(p, 'fs') for p in packed[:2])  24 us
    all_gather x1, blocking collectives, local(): latents = lax.all_gather(latents, 'tp')  21.2 us
    all_gather x1, blocking collectives, local(): stats = lax.all_gather(stats, 'tp')  19.2 us
    all_gather x1, blocking collectives, local(): narrow_all = lax.all_gather(narrow, 'fs')  12.8 us
    all_gather x1, blocking collectives, local(): third_all = lax.all_gather(packed[2], 'fs')  11.1 us
    all_gather x1, blocking collectives, local(): mine = lax.all_gather(share, 'tp', axis_index_groups=SAME_CORE)  10.1 us
    ppermute x1, starting transfers between devices, local(): other = lax.ppermute(mine, 'tp', CORE_PAIRS)  6.26 us
  transfers between devices with their start and end apart: 3, of which 2 were waited for; matrix products, arithmetic and copies ran while one was open for 0% of the time, Pallas kernels for 3%

profile of v2, /device:TPU:1, one launch (start us, length us, event | category | flops | bytes accessed | tf_op | source)
XLA Modules:
  0.0 168.5 jit_solution(3879031184446261408)
XLA Ops:
  6.5 0.0 copy-start.5
  6.5 0.0 copy-start
  6.5 0.0 all-gather.10.cloned.1.call-start
  6.6 1.1 shard_map.181
  7.6 12.8 %all-gather = bf16[896,512]{1,0:T(8,128)(2,1)S(1)} all-gather(bf16[224,512]{1,0:T(8,128)(2,1)S(1)} %get-tuple-element.29), channel_id=2, replica_groups=mesh['sp'=16,'fs'=4,'tp'=8] {'fs'}, dimensions={0}, use_global_device_ids=true | all-gather | bytes 1146880 | tf_op jit(solution)/shard_map/all_gather | solution.py:421
  20.4 0.1 multiply_sine_fusion
  20.6 2.3 %shard_map.182 = (bf16[320,128]{1,0:T(8,128)(2,1)S(1)}, bf16[256,128]{1,0:T(8,128)(2,1)S(1)}, bf16[256,2048]{1,0:T(8,128)(2,1)S(1)}, f32[256,128]{1,0:T(8,128)S(...) custom-call(bf16[256,2048]{1,0:T(8,128)(2,1)} %bitcast.39, f32[1,2048]{1,0:T(1,128)S(1)} %get-tuple-element.27.gain_ref, ...), custom_call_target="tpu_custom_call" | custom-call | tf_op jit(solution)/shard_map/pallas_call | solution.py:425
  22.9 21.2 %all-gather.1 = bf16[2560,128]{1,0:T(8,128)(2,1)S(1)} all-gather(bf16[320,128]{1,0:T(8,128)(2,1)S(1)} %get-tuple-element.30), channel_id=3, replica_groups=mesh['sp'=16,'fs'=4,'tp'=8] {'tp'}, dimensions={0}, use_global_device_ids=true | all-gather | bytes 737280 | tf_op jit(solution)/shard_map/all_gather | solution.py:438
  44.1 0.0 copy-done.5
  44.1 0.0 copy-done
  44.1 2.1 %shard_map.183.own_ref = bf16[768,128]{1,0:T(8,128)(2,1)} custom-call(bf16[8,320,128]{2,1,0:T(8,128)(2,1)S(1)} %bitcast.29, bf16[256,128]{1,0:T(8,128)(2,1)S(1)} %get-tuple-element.31.rope_ref, bf16[4,224,512]{2,1,0:T(8,128)(2,1)S(1)} %bitcast.26, f32[1,512]{1,0:T(1,128)S(1)} %bitcast.35, f32[1,128]{1,0:T(1,128)S(1)} %pad_bitcast_fusion.1.kgain_ref, ...), custom_call_target="tpu_custom_call" | custom-call | tf_op jit(solution)/shard_map/pallas_call | solution.py:443
  46.2 0.0 copy-start.3
  46.2 0.0 all-gather.10.cloned.1.call-update
  46.2 1.2 shard_map.184
  47.4 0.0 copy-start.6
  47.4 0.0 copy-start.4
  47.4 11.5 %all-gather.4 = bf16[768,512]{1,0:T(8,128)(2,1)S(1)} all-gather(bf16[192,512]{1,0:T(8,128)(2,1)S(1)} %get-tuple-element.45), channel_id=6, replica_groups=mesh['sp'=16,'fs'=4,'tp'=8] {'fs'}, dimensions={0}, use_global_device_ids=true | all-gather | bytes 983040 | tf_op jit(solution)/shard_map/all_gather | solution.py:461
  58.9 12.5 %all-gather.2 = bf16[896,512]{1,0:T(8,128)(2,1)S(1)} all-gather(bf16[224,512]{1,0:T(8,128)(2,1)S(1)} %get-tuple-element.40), channel_id=4, replica_groups=mesh['sp'=16,'fs'=4,'tp'=8] {'fs'}, dimensions={0}, use_global_device_ids=true | all-gather | bytes 1146880 | tf_op jit(solution)/shard_map/all_gather | solution.py:461
  71.4 0.0 copy-start.1
  71.4 0.0 copy-start.2
  71.4 0.7 shard_map.187.gated_ref
  72.2 1.3 collective-permute-start
  73.5 0.0 copy-done.3
  73.5 11.1 %all-gather.6 = bf16[768,512]{1,0:T(8,128)(2,1)S(1)} all-gather(bf16[192,512]{1,0:T(8,128)(2,1)S(1)} %get-tuple-element.48), channel_id=8, replica_groups=mesh['sp'=16,'fs'=4,'tp'=8] {'fs'}, dimensions={0}, use_global_device_ids=true | all-gather | bytes 983040 | tf_op jit(solution)/shard_map/all_gather | solution.py:486
  84.6 0.0 copy-done.6
  84.6 0.0 copy-done.4
  84.6 1.3 shard_map.185.q_ref
  85.9 1.7 shard_map.186
  87.5 0.0 collective-permute-done.halo_ref
  87.5 0.4 shard_map.188
  88.0 19.2 %all-gather.5 = f32[64,128]{1,0:T(8,128)S(1)} all-gather(f32[8,128]{1,0:T(8,128)S(1)} %get-tuple-element.47), channel_id=7, replica_groups=mesh['sp'=16,'fs'=4,'tp'=8] {'tp'}, dimensions={0}, use_global_device_ids=true | all-gather | bytes 36864 | tf_op jit(solution)/shard_map/all_gather | solution.py:478
  107.2 0.0 copy-done.1
  107.2 0.0 copy-done.2
  107.2 0.2 shard_map.189.conv_ref
  107.4 4.5 %all-gather.10.cloned.1.call-done = bf16[12288,128]{1,0:T(8,128)(2,1)} async-done(((bf16[768,128]{1,0:T(8,128)(2,1)}), bf16[12288,128]{1,0:T(8,128)(2,1)}) %all-gather.10.cloned.1.call-update) | async-done | bytes 3145744 | tf_op jit(solution)/shard_map/all_gather | solution.py:454
  111.9 2.4 %shard_map.190 = bf16[8,32,2048]{2,1,0:T(8,128)(2,1)S(1)} custom-call(s32[1]{0:T(128)} %bitcast.1.at_ref, bf16[256,256]{1,0:T(8,128)(2,1)S(1)} %shard_map.185.q_ref, bf16[4,4,768,128]{3,2,1,0:T(8,128)(2,1)} %bitcast.38, f32[8,256]{1,0:T(8,128)S(1)} %get-tuple-element.42.stat_ref, f32[128,256]{1,0:T(8,128)S(1)} %get-tuple-element.43.acc_ref, ...), custom_call_target="tpu_custom_call" | custom-call | tf_op jit(solution)/shard_map/pallas_call | solution.py:491
  114.2 28.4 %all_to_all.5.in_ref = bf16[8,32,2048]{2,1,0:T(8,128)(2,1)S(1)} all-to-all(bf16[8,32,2048]{2,1,0:T(8,128)(2,1)S(1)} %shard_map.190), channel_id=1, replica_groups=mesh['sp'=16,'fs'=4,'tp'=8] {'tp'}, dimensions={0} | all-to-all | bytes 2097152 | tf_op jit(solution)/shard_map/all_to_all | solution.py:502
  142.7 0.1 shard_map.191
  142.8 10.1 %all-gather.7 = bf16[128,2048]{1,0:T(8,128)(2,1)S(1)} all-gather(bf16[32,2048]{1,0:T(8,128)(2,1)S(1)} %shard_map.191), channel_id=9, replica_groups={{0,2,4,6},{1,3,5,7},{8,10,12,14},{9,11,13,15},{16,18,20,22},{17,19,21,2..., dimensions={0}, use_global_device_ids=true | all-gather | bytes 655360 | tf_op jit(solution)/shard_map/all_gather | solution.py:504
  152.8 6.3 %collective-permute-start.1 = (bf16[4,32,2048]{2,1,0:T(8,128)(2,1)S(1)}, bf16[4,32,2048]{2,1,0:T(8,128)(2,1)S(1)}, u32[]{:S(2)}, u32[]{:S(2)}) collective-permute-start(bf16[4,32,2048]{2,1,0:T(8,128)(2,1)S(1)} %bitcast.32), channel_id=1, source_target_pairs={{0,1},{1,0},{2,3},{3,2},{4,5},{5,4},{6,7},{7,6},{8,9},{9,8},{10,11... | collective-permute-start | bytes 1572872 | tf_op jit(solution)/shard_map/ppermute | solution.py:505
  159.1 1.5 collective-permute-done.1.other_ref
  160.6 1.0 shard_map.192
  (7 shorter events, 0.0 us)
Async XLA Ops:
  6.5 37.5 %copy-start.5 = (f32[96]{0:T(128)S(1)}, f32[96]{0:T(128)}, u32[]{:S(2)}) copy-start(f32[96]{0:T(128)} %param.30) | copy-start | bytes 1156
  6.5 37.5 %copy-start = (f32[512]{0:T(512)S(1)}, f32[512]{0:T(512)}, u32[]{:S(2)}) copy-start(f32[512]{0:T(512)} %param.28) | copy-start | bytes 6148
  6.5 105.3 %all-gather.10.cloned.1.call-start = ((), (), s32[]{:S(2)}) async-start(), calls=%async_computation.1 | async-start | bytes 3342336 | tf_op jit(solution)/shard_map/all_gather | solution.py:454
  46.2 27.3 %copy-start.3 = (bf16[31,128]{1,0:T(8,128)(2,1)S(1)}, bf16[31,128]{1,0:T(8,128)(2,1)}, u32[]{:S(2)}) copy-start(bf16[31,128]{1,0:T(8,128)(2,1)} %param.33) | copy-start | bytes 23812
  47.4 37.1 %copy-start.6 = (f32[96]{0:T(128)S(1)}, f32[96]{0:T(128)}, u32[]{:S(2)}) copy-start(f32[96]{0:T(128)} %param.29) | copy-start | bytes 1156
  47.4 37.1 %copy-start.4 = (f32[768]{0:T(1024)S(1)}, f32[768]{0:T(1024)}, u32[]{:S(2)}) copy-start(f32[768]{0:T(1024)} %param.27) | copy-start | bytes 9220
  71.4 35.7 %copy-start.1 = (f32[128]{0:T(128)S(1)}, f32[128]{0:T(128)}, u32[]{:S(2)}) copy-start(f32[128]{0:T(128)} %param.34) | copy-start | bytes 1540
  71.4 35.7 %copy-start.2 = (f32[128]{0:T(128)S(1)}, f32[128]{0:T(128)}, u32[]{:S(2)}) copy-start(f32[128]{0:T(128)} %param.35) | copy-start | bytes 1540
  72.2 15.4 %collective-permute-start = (bf16[32,128]{1,0:T(8,128)(2,1)S(1)}, bf16[32,128]{1,0:T(8,128)(2,1)S(1)}, u32[]{:S(2)}, u32[]{:S(2)}) collective-permute-start(bf16[32,128]{1,0:T(8,128)(2,1)S(1)} %slice.4), channel_id=1, source_target_pairs={{0,32},{32,64},{64,96},{96,128},{128,160},{160,192},{192,224},{224... | collective-permute-start | bytes 24584 | tf_op jit(solution)/shard_map/ppermute | solution.py:471
  152.8 7.8 %collective-permute-start.1 = (bf16[4,32,2048]{2,1,0:T(8,128)(2,1)S(1)}, bf16[4,32,2048]{2,1,0:T(8,128)(2,1)S(1)}, u32[]{:S(2)}, u32[]{:S(2)}) collective-permute-start(bf16[4,32,2048]{2,1,0:T(8,128)(2,1)S(1)} %bitcast.32), channel_id=1, source_target_pairs={{0,1},{1,0},{2,3},{3,2},{4,5},{5,4},{6,7},{7,6},{8,9},{9,8},{10,11... | collective-permute-start | bytes 1572872 | tf_op jit(solution)/shard_map/ppermute | solution.py:505
Sparse Core Ops, SparseCore 0:
  46.3 65.5 all-gather.9
